TPU v7x, 32 devices: a whole 2x2x4 slice. The times are simulated.
32 devices in a mesh: sp: 8 (over z, y), tp: 4 (over x, core).
Axes of the slice: x: 2, y: 2, z: 4, core: 2. Of those that a mesh axis runs over, the one named last changes fastest.
Arguments:
- arriving_hidden_state: bfloat16 [8192, 2048], P(('sp', 'tp')), may hold values from -6 to 6
- former_request_vectors: bfloat16 [8192, 1024], P('sp', 'tp'), may hold values from -6 to 6
- former_match_vectors: bfloat16 [8192, 1024], P('sp', 'tp'), may hold values from -6 to 6
- latter_request_vectors: bfloat16 [8192, 512], P('sp', 'tp'), may hold values from -6 to 6
- latter_match_vectors: bfloat16 [8192, 512], P('sp', 'tp'), may hold values from -6 to 6
- stored_vectors_both: bfloat16 [8192, 2, 1024], P('sp', None, 'tp'), may hold values from -6 to 6
- closing_valve_operands: bfloat16 [8192, 2, 1024], P('sp', None, 'tp'), may hold values from -6 to 6
- update_level_before_squash: bfloat16 [2, 8, 8192], P(None, 'tp', 'sp'), may hold values from -4 to -3
- fading_data_input: float32 [2, 8, 8192], P(None, 'tp', 'sp'), may hold values from -5.5 to 5.5
- sparse_fading_boost: float32 [2, 8, 8192], P(None, 'tp', 'sp'), may hold values from -2 to 0, as said below
- unitwise_fading_loglevel: float32 [2, 8], P(None, 'tp'), as said below
- fading_constant_term: float32 [2, 8], P(None, 'tp'), may hold values from -1 to 1
- unitwise_normalizer_coef: float32 [128], replicated, may hold values from 0.1 to 1.9
- emission_map_weights: bfloat16 [2048, 2048], replicated, may hold values from -0.125 to 0.125
- channel_normalizer_coef: float32 [2048], replicated, may hold values from 0.1 to 1.9
- switching_channel_map: bfloat16 [2048, 6144], P('sp', 'tp'), may hold values from -0.125 to 0.125
- broadening_channel_map: bfloat16 [2048, 6144], P('sp', 'tp'), may hold values from -0.125 to 0.125
- timewise_convolve_tapvalues: bfloat16 [3, 2, 6144], P(None, None, 'tp'), may hold values from -3.5 to 3.5
- narrowing_map_weights_in: bfloat16 [2048, 6144], P('sp', 'tp'), may hold values from -0.078125 to 0.078125
Outputs:
- mixed: bfloat16 [8192, 2048], P(('sp', 'tp'))
Inputs may be any that keep to these rules, and one draw needn't show every extreme that they name: `unitwise_fading_loglevel`: each entry is the logarithm of a per-position rate between 0.2 / 8192 and 2 / 64. `sparse_fading_boost`: zero except at three or fewer positions of the sequence.
All inputs are finite; a program needn't handle non-finite values.
Results may differ from a plain program's by a relative error of at most 0.015.
Values may be sent and summed in bfloat16 or wider, within the bound.
A program may use at most 128 MiB of HBM per device.

v0:
```python
import jax
import jax.numpy as jnp
from jax import lax
from jax.sharding import PartitionSpec as P

SPAN = 64
TAPS = 3


EPSILON = 1e-06
PRECISE = lax.Precision.HIGHEST


def prefix(shard, axis, join, neutral):
    place = lax.axis_index(axis)
    gathered = jax.tree.map(
        lambda a, kind: lax.all_gather(a.astype(kind), axis),
        shard,
        (jnp.bfloat16, jnp.bfloat16, jnp.bfloat16, jnp.bfloat16),
    )
    state = jax.tree.map(lambda a, e: jnp.zeros_like(a) + jnp.asarray(e, a.dtype), shard, neutral)

    def one(turn, state):
        return join(
            state,
            jax.tree.map(
                lambda a, own: lax.dynamic_index_in_dim(a, turn, 0, False).astype(own.dtype),
                gathered,
                shard,
            ),
        )

    return lax.fori_loop(0, place, one, state)


def from_behind(value, axis, steps):
    count = lax.axis_size(axis)
    leading, last = (max(0, -steps), min(count, count - steps))
    return lax.ppermute(value, axis, [(source, source + steps) for source in range(leading, last)])


def unit_rows(matrix):
    return matrix * lax.rsqrt(jnp.sum(matrix * matrix, axis=-1, keepdims=True) + EPSILON)


def heads_first(matrix, head_count):
    row_count = matrix.shape[0]
    return matrix.reshape(row_count, head_count, -1).astype(jnp.float32).transpose(1, 0, 2)


def block_terms(queries, key_rows, value_rows, beta_rate, gate_logarithms):
    head_count, length, key_size = queries.shape
    num_blocks = length // SPAN
    queries = queries.reshape(head_count, num_blocks, SPAN, -1)
    key_rows = key_rows.reshape(head_count, num_blocks, SPAN, -1)
    value_rows = value_rows.reshape(head_count, num_blocks, SPAN, -1)
    beta_rate = beta_rate.reshape(head_count, num_blocks, SPAN)
    cum_gates = jnp.cumsum(gate_logarithms.reshape(head_count, num_blocks, SPAN), axis=-1)
    row_pos = lax.broadcasted_iota(jnp.int32, (SPAN, SPAN), 0)
    col_pos = lax.broadcasted_iota(jnp.int32, (SPAN, SPAN), 1)
    causal = row_pos >= col_pos
    strict = row_pos > col_pos
    decay = jnp.exp(jnp.where(causal, cum_gates[..., :, None] - cum_gates[..., None, :], -jnp.inf))
    key_beta = key_rows * beta_rate[..., None]
    lower = jnp.where(
        strict, jnp.einsum("hncd,hnsd->hncs", key_beta, key_rows, precision=PRECISE) * decay, 0.0
    )
    right_side = jnp.concatenate(
        [value_rows * beta_rate[..., None], key_beta * jnp.exp(cum_gates)[..., None]], axis=-1
    )
    unit_mat = jnp.eye(SPAN, dtype=lower.dtype)
    solved = lax.linalg.triangular_solve(
        lower + unit_mat, right_side, left_side=True, lower=True, unit_diagonal=True
    )
    value_size = value_rows.shape[-1]
    u_values = solved[..., :value_size]
    w_keys = solved[..., value_size:]
    intra = jnp.einsum("hncd,hnsd->hncs", queries, key_rows, precision=PRECISE) * decay
    key_decayed = key_rows * jnp.exp(cum_gates[..., -1:] - cum_gates)[..., None]
    return (queries, u_values, w_keys, intra, key_decayed, cum_gates)


def run_blocks(increment_list, initial_memory):

    def run_advance(state_mat, inputs):
        query_blk, u_blk, w_blk, intra_blk, kdec_blk, cum_blk = inputs
        fresh = u_blk - jnp.einsum("hcd,hde->hce", w_blk, state_mat, precision=PRECISE)
        output = jnp.einsum(
            "hcd,hde->hce", query_blk * jnp.exp(cum_blk)[..., None], state_mat, precision=PRECISE
        )
        output = output + jnp.einsum("hcs,hse->hce", intra_blk, fresh, precision=PRECISE)
        state_mat = state_mat * jnp.exp(cum_blk[:, -1])[:, None, None]
        state_mat = state_mat + jnp.einsum("hcd,hce->hde", kdec_blk, fresh, precision=PRECISE)
        return (state_mat, output)

    moved = tuple((jnp.moveaxis(member, 1, 0) for member in increment_list))
    _, outputs = lax.scan(run_advance, initial_memory, moved)
    head_count = outputs.shape[1]
    return jnp.moveaxis(outputs, 0, 1).reshape(head_count, -1, outputs.shape[-1])


def summarize(increment_list):
    queries, u_values, w_keys, intra, key_decayed, cum_gates = increment_list
    head_count, num_blocks, span_len, key_size = key_decayed.shape
    value_size = u_values.shape[-1]
    unit_mat = jnp.eye(key_size, dtype=jnp.float32)
    last_decay = jnp.exp(cum_gates[..., -1])[..., None, None]
    step_maps = last_decay * unit_mat - jnp.einsum(
        "hncd,hnce->hnde", key_decayed, w_keys, precision=PRECISE
    )
    step_adds = jnp.einsum("hncd,hnce->hnde", key_decayed, u_values, precision=PRECISE)

    def summarize_advance(running, inputs):
        block_map, block_add = inputs
        new_map = jnp.einsum("hij,hjk->hik", block_map, running[0], precision=PRECISE)
        new_add = jnp.einsum("hij,hjk->hik", block_map, running[1], precision=PRECISE) + block_add
        return ((new_map, new_add), None)

    initial = (
        jnp.broadcast_to(unit_mat, (head_count, key_size, key_size)),
        jnp.zeros((head_count, key_size, value_size), jnp.float32),
    )
    (total_map, total_add), _ = lax.scan(
        summarize_advance, initial, (jnp.moveaxis(step_maps, 1, 0), jnp.moveaxis(step_adds, 1, 0))
    )
    return (total_map, total_add)


def apply_map(map_flat, other_flat, key_size, col_count):
    head_count = map_flat.shape[0]
    product = jnp.einsum(
        "hij,hjk->hik",
        map_flat.reshape(head_count, key_size, key_size),
        other_flat.reshape(head_count, key_size, col_count),
        precision=PRECISE,
    )
    return product.reshape(head_count, -1)


def team_parts(
    asker_weights,
    lookup_weights,
    value_matrix,
    correction_draw,
    decay_draw,
    spike_draw,
    decay_logarithm,
    bias_vector,
):
    head_count = decay_logarithm.shape[0]
    queries = heads_first(asker_weights, head_count)
    key_size = queries.shape[-1]
    queries = unit_rows(queries) * key_size ** (-0.5)
    key_rows = unit_rows(heads_first(lookup_weights, head_count))
    value_rows = heads_first(value_matrix, head_count)
    beta_rate = jax.nn.sigmoid(correction_draw.astype(jnp.float32))
    gate_logarithms = (
        -jnp.exp(decay_logarithm)[:, None] * jax.nn.softplus(decay_draw + bias_vector[:, None])
        + spike_draw
    )
    return block_terms(queries, key_rows, value_rows, beta_rate, gate_logarithms)


def completed_attn_units(increment_list, initial_memory, gate_cols, unitwise_normalizer_coef):
    outputs = run_blocks(increment_list, initial_memory)
    head_count = outputs.shape[0]
    gates_in = heads_first(gate_cols, head_count)
    scaled = (
        outputs
        * lax.rsqrt(jnp.mean(outputs * outputs, axis=-1, keepdims=True) + EPSILON)
        * unitwise_normalizer_coef
    )
    scaled = scaled * jax.nn.silu(gates_in)
    return scaled.transpose(1, 0, 2).reshape(outputs.shape[1], -1).astype(jnp.bfloat16)


def causal_taps(edge_rows, low_rows, taps_col):
    padded = jnp.concatenate([edge_rows, low_rows], axis=0)
    length = low_rows.shape[0]
    total = taps_col[0] * padded[0:length]
    for tap_index in range(1, TAPS):
        total = total + taps_col[tap_index] * padded[tap_index : tap_index + length]
    return total


def per_device(
    arriving_hidden_state,
    former_request_vectors,
    former_match_vectors,
    latter_request_vectors,
    latter_match_vectors,
    stored_vectors_both,
    closing_valve_operands,
    update_level_before_squash,
    fading_data_input,
    sparse_fading_boost,
    unitwise_fading_loglevel,
    fading_constant_term,
    unitwise_normalizer_coef,
    emission_map_weights,
    channel_normalizer_coef,
    switching_channel_map,
    broadening_channel_map,
    timewise_convolve_tapvalues,
    narrowing_map_weights_in,
):
    whole_gate, whole_up, whole_down = (
        lax.all_gather(switching_channel_map, "sp", axis=0, tiled=True),
        lax.all_gather(broadening_channel_map, "sp", axis=0, tiled=True),
        lax.all_gather(narrowing_map_weights_in, "sp", axis=0, tiled=True),
    )
    increments_former = team_parts(
        former_request_vectors,
        former_match_vectors,
        stored_vectors_both[:, 0],
        update_level_before_squash[0],
        fading_data_input[0],
        sparse_fading_boost[0],
        unitwise_fading_loglevel[0],
        fading_constant_term[0],
    )
    increments_latter = team_parts(
        latter_request_vectors,
        latter_match_vectors,
        stored_vectors_both[:, 1],
        update_level_before_squash[1],
        fading_data_input[1],
        sparse_fading_boost[1],
        unitwise_fading_loglevel[1],
        fading_constant_term[1],
    )
    map_one, add_one = summarize(increments_former)
    map_two, add_two = summarize(increments_latter)
    head_count = map_one.shape[0]
    size_one = map_one.shape[-1]
    size_two = map_two.shape[-1]
    value_size = add_one.shape[-1]
    flat_one = map_one.reshape(head_count, -1)
    flat_add_one = add_one.reshape(head_count, -1)
    flat_two = map_two.reshape(head_count, -1)
    flat_add_two = add_two.reshape(head_count, -1)

    def compose(earlier, later):
        return (
            apply_map(later[0], earlier[0], size_one, size_one),
            apply_map(later[0], earlier[1], size_one, value_size) + later[1],
            apply_map(later[2], earlier[2], size_two, size_two),
            apply_map(later[2], earlier[3], size_two, value_size) + later[3],
        )

    identity = (
        jnp.broadcast_to(jnp.eye(size_one, dtype=jnp.float32).reshape(1, -1), flat_one.shape),
        jnp.zeros(flat_add_one.shape, jnp.float32),
        jnp.broadcast_to(jnp.eye(size_two, dtype=jnp.float32).reshape(1, -1), flat_two.shape),
        jnp.zeros(flat_add_two.shape, jnp.float32),
    )
    before = prefix((flat_one, flat_add_one, flat_two, flat_add_two), "sp", compose, identity)
    initial_former = before[1].reshape(head_count, size_one, value_size)
    initial_latter = before[3].reshape(head_count, size_two, value_size)
    heads_one = completed_attn_units(
        increments_former, initial_former, closing_valve_operands[:, 0], unitwise_normalizer_coef
    )
    heads_two = completed_attn_units(
        increments_latter, initial_latter, closing_valve_operands[:, 1], unitwise_normalizer_coef
    )
    linear_attend = jnp.stack([heads_one, heads_two], axis=1)
    arrived = lax.all_to_all(linear_attend, "tp", split_axis=0, concat_axis=2, tiled=True)
    row_count = arrived.shape[0]
    skip_stream = arriving_hidden_state.astype(jnp.float32) + jnp.dot(
        arrived.reshape(row_count, -1), emission_map_weights, preferred_element_type=jnp.float32
    )
    normed = (
        skip_stream
        * lax.rsqrt(jnp.mean(skip_stream * skip_stream, axis=-1, keepdims=True) + EPSILON)
        * channel_normalizer_coef
    ).astype(jnp.bfloat16)
    features = lax.all_gather(normed, "tp", axis=0, tiled=True)
    gate_full = jnp.dot(features, whole_gate, preferred_element_type=jnp.float32)
    up_full = jnp.dot(features, whole_up, preferred_element_type=jnp.float32)
    gate_low = gate_full.astype(jnp.bfloat16)
    up_low = up_full.astype(jnp.bfloat16)
    edge_gate, edge_up = from_behind((gate_low[-(TAPS - 1) :], up_low[-(TAPS - 1) :]), "sp", 1)
    taps = timewise_convolve_tapvalues.astype(jnp.float32)
    gate_conv = causal_taps(edge_gate, gate_low, taps[:, 0])
    up_conv = causal_taps(edge_up, up_low, taps[:, 1])
    hidden = (jax.nn.silu(gate_conv) * up_conv).astype(jnp.bfloat16)
    down_sum = lax.psum_scatter(
        lax.dot_general(
            hidden, whole_down, (((1,), (1,)), ((), ())), preferred_element_type=jnp.float32
        ).astype(jnp.bfloat16),
        "tp",
        scatter_dimension=0,
        tiled=True,
    ).astype(jnp.float32)
    return (skip_stream + down_sum).astype(jnp.bfloat16)


def solution(mesh):
    placed = (
        P(("sp", "tp"), None),
        P("sp", "tp"),
        P("sp", "tp"),
        P("sp", "tp"),
        P("sp", "tp"),
        P("sp", None, "tp"),
        P("sp", None, "tp"),
        P(None, "tp", "sp"),
        P(None, "tp", "sp"),
        P(None, "tp", "sp"),
        P(None, "tp"),
        P(None, "tp"),
        P(),
        P(),
        P(),
        P("sp", "tp"),
        P("sp", "tp"),
        P(None, None, "tp"),
        P("sp", "tp"),
    )
    return jax.shard_map(
        per_device, mesh=mesh, in_specs=placed, out_specs=P(("sp", "tp"), None), check_vma=False
    )
```

profile of v0, /device:TPU:0, one launch (start us, length us, event | category | flops | bytes accessed | tf_op | source)
XLA Modules:
  0.0 1172.6 jit_solution(12916123732911664688)
XLA Ops:
  15.5 2.9 fusion.91
  18.4 158.0 %custom-call.7 = f32[2,16,1,64,64]{3,4,2,1,0:T(8,128)S(1)} custom-call(f32[2,16,1,64,64]{4,3,2,1,0:T(8,128)} %fusion.91), custom_call_target="InvertDiagBlocksLowerTriangular" | custom-call | tf_op jit(solution)/shard_map/triangular_solve | solution.py:72
  176.4 2.4 slice_convert_fusion
  179.3 1.8 multiply_bitcast_fusion
  181.1 2.0 fusion.62
  183.1 3.2 convolution_bitcast_fusion.5
  189.2 1.3 copy.119
  190.5 3.7 fusion.106
  194.2 158.7 %custom-call.6 = f32[2,16,1,64,64]{3,4,2,1,0:T(8,128)} custom-call(f32[2,16,1,64,64]{4,3,2,1,0:T(8,128)} %fusion.106), custom_call_target="InvertDiagBlocksLowerTriangular" | custom-call | tf_op jit(solution)/shard_map/triangular_solve | solution.py:72
  352.9 2.1 multiply_bitcast_fusion.1
  355.0 2.0 fusion.58
  357.0 5.1 convolution_bitcast_fusion.2
  362.2 1.6 slice_bitcast_fusion.3
  363.8 2.2 fusion.78
  366.1 20.8 %while.69 = (s32[]{:T(128)}, f32[2,64,64]{2,1,0:T(8,128)S(1)}, f32[2,64,128]{2,1,0:T(8,128)S(1)}, f32[16,2,64,64]{3,2,0,1:T(8,128)S(1)}, f32[16,2,64,128]{3,2,0,1:T(8,128)}, /*index=5*/s32[]{:T(128)}, s32[]{:T(128)}) while((s32[]{:T(128)}, f32[2,64,64]{2,1,0:T(8,128)S(1)}, f32[2,64,128]{2,1,0:T(8,128)S(1)}, ...), condition=%wide.region_7.8_spmd.clone, body=%wide.region_6.7_spmd.clone.sunk | while | flops 18907140 | bytes 623707 | solution.py:123
  386.9 34.6 %all_gather.31 = bf16[8,2,8192]{2,1,0:T(2,128)(2,1)} all-gather(bf16[1,2,8192]{2,1,0:T(2,128)(2,1)S(1)} %convert_element_type.237), channel_id=1, replica_groups=mesh['sp'=8,'tp'=4] {'sp'}, dimensions={0}, use_global_device_ids=true | all-gather | bytes 294912 | tf_op jit(solution)/shard_map/all_gather | solution.py:17
  421.6 32.6 %all_gather.30 = bf16[8,2,4096]{2,1,0:T(2,128)(2,1)} all-gather(bf16[1,2,4096]{2,1,0:T(2,128)(2,1)S(1)} %convert_element_type.235), channel_id=1, replica_groups=mesh['sp'=8,'tp'=4] {'sp'}, dimensions={0}, use_global_device_ids=true | all-gather | bytes 147456 | tf_op jit(solution)/shard_map/all_gather | solution.py:17
  454.1 6.5 bitcast_subtract_fusion
  460.6 39.9 %while.68 = (s32[]{:T(128)}, f32[2,128,128]{2,1,0:T(8,128)S(1)}, f32[2,128,128]{2,1,0:T(8,128)S(1)}, f32[16,2,128,128]{3,2,0,1:T(8,128)}, f32[16,2,128,128]{3,2,0,1:T(8,128)}, /*index=5*/s32[]{:T(128)}, s32[]{:T(128)}) while((s32[]{:T(128)}, f32[2,128,128]{2,1,0:T(8,128)S(1)}, f32[2,128,128]{2,1,0:T(8,128)S(1)}, ...), condition=%wide.region_3.4_spmd.clone, body=%wide.region_2.3_spmd.clone.sunk | while | flops 100728832 | bytes 1443415 | solution.py:123
  500.6 31.6 %all_gather.28 = bf16[8,2,16384]{2,1,0:T(2,128)(2,1)S(1)} all-gather(bf16[1,2,16384]{2,1,0:T(2,128)(2,1)S(1)} %convert_element_type.228), channel_id=1, replica_groups=mesh['sp'=8,'tp'=4] {'sp'}, dimensions={0}, use_global_device_ids=true | all-gather | bytes 589824 | tf_op jit(solution)/shard_map/all_gather | solution.py:17
  532.2 31.2 %all_gather.29 = bf16[8,2,16384]{2,1,0:T(2,128)(2,1)S(1)} all-gather(bf16[1,2,16384]{2,1,0:T(2,128)(2,1)S(1)} %convert_element_type.230), channel_id=1, replica_groups=mesh['sp'=8,'tp'=4] {'sp'}, dimensions={0}, use_global_device_ids=true | all-gather | bytes 589824 | tf_op jit(solution)/shard_map/all_gather | solution.py:17
  565.8 1.3 reshape.410
  567.1 3.2 fusion.76
  570.5 62.9 %while.67 = (s32[]{:T(128)}, f32[2,64,128]{2,1,0:T(8,128)S(1)}, f32[16,2,64,128]{3,2,0,1:T(8,128)S(1)}, f32[16,2,64]{2,0,1:T(8,128)S(1)}, f32[16,2,64,64]{3,2,0,...) while((s32[]{:T(128)}, f32[2,64,128]{2,1,0:T(8,128)S(1)}, ...), condition=%wide.region_16.17_spmd, body=%wide.region_15.16_spmd.sunk | while | flops 50405376 | bytes 1086597 | solution.py:97
  636.4 1.5 copy.132
  637.9 2.7 fusion.77
  640.8 63.3 %while.66 = (s32[]{:T(128)}, f32[2,128,128]{2,1,0:T(8,128)S(1)}, f32[16,2,64,128]{3,2,0,1:T(8,128)S(1)}, f32[16,2,64]{2,0,1:T(8,128)S(1)}, f32[16,2,64,128]{3,2,...) while((s32[]{:T(128)}, f32[2,128,128]{2,1,0:T(8,128)S(1)}, ...), condition=%wide.region_12.13_spmd, body=%wide.region_11.12_spmd.sunk | while | flops 88195072 | bytes 1250949 | solution.py:97
  647.4 1.3 convolution_add_fusion.11
  651.4 1.3 convolution_add_fusion.11
  704.6 4.1 fusion.165
  708.7 2.3 copy.182
  712.2 3.5 copy.183
  715.7 2.2 copy.153
  717.9 2.6 fusion.117
  724.1 17.2 %all_to_all.15 = bf16[1024,2,256]{2,1,0:T(2,128)(2,1)S(1)} all-to-all(bf16[1024,2,256]{2,1,0:T(2,128)(2,1)S(1)} %copy.155), channel_id=1, replica_groups=mesh['sp'=8,'tp'=4] {'tp'}, dimensions={0} | all-to-all | bytes 2097152 | tf_op jit(solution)/shard_map/all_to_all | solution.py:267
  742.0 6.1 multiply_reduce_fusion
  751.5 48.4 %all-gather.5.cloned.1.call-done = bf16[1024,2048]{1,0:T(8,128)(2,1)} async-done(((bf16[256,2048]{1,0:T(8,128)(2,1)}), bf16[1024,2048]{1,0:T(8,128)(2,1)}) %all-gather.5.cloned.1.call-update) | async-done | bytes 4194320 | tf_op jit(solution)/shard_map/all_gather | solution.py:277
  799.8 100.9 %all-gather.7.cloned.1.call-done = bf16[2048,1536]{1,0:T(8,128)(2,1)} async-done(((bf16[256,1536]{1,0:T(8,128)(2,1)}), bf16[2048,1536]{1,0:T(8,128)(2,1)}) %all-gather.7.cloned.1.call-update) | async-done | bytes 6291472 | tf_op jit(solution)/shard_map/all_gather | solution.py:208
  900.8 10.0 convolution_convert_fusion.2
  910.8 1.6 copy-done.22
  912.4 2.4 collective-permute-start
  914.9 85.1 %all-gather.9.cloned.1.call-done = bf16[2048,1536]{1,0:T(8,128)(2,1)} async-done(((bf16[256,1536]{1,0:T(8,128)(2,1)}), bf16[2048,1536]{1,0:T(8,128)(2,1)}) %all-gather.9.cloned.1.call-update) | async-done | bytes 6291472 | tf_op jit(solution)/shard_map/all_gather | solution.py:209
  1000.0 10.0 convolution_convert_fusion.1
  1010.0 2.7 collective-permute-start.1
  1012.8 86.2 %all-gather.11.cloned.1.call-done = bf16[2048,1536]{1,0:T(8,128)(2,1)} async-done(((bf16[256,1536]{1,0:T(8,128)(2,1)}), bf16[2048,1536]{1,0:T(8,128)(2,1)}) %all-gather.11.cloned.1.call-update) | async-done | bytes 6291472 | tf_op jit(solution)/shard_map/all_gather | solution.py:210
  1099.1 21.2 %convolution_convert_fusion = bf16[1024,2048]{1,0:T(8,128)(2,1)} fusion(bf16[2048,1536]{1,0:T(8,128)(2,1)} %all-gather.11.cloned.1.call-done, bf16[1024,1536]{1,0:T(8,128)(2,1)} %copy-done.23, bf16[1024,1536]{1,0:T(8,128)(2,1)} %copy-done.22, bf16[2,1536]{1,0:T(2,128)(2,1)S(1)} %collective-permute-done.1, bf16[2,1536]{1,0:T(2,128)(2,1)S(1)} %collective-permute-done, ...), kind=kOutput, calls=%fused_computation.78 | convolution fusion | flops 6498025472 | bytes 16826368 | tf_op jit(solution)/shard_map/dot_general | solution.py:288
  1120.3 42.9 %reduce-scatter.2.cloned.1.call-done = bf16[256,2048]{1,0:T(8,128)(2,1)} async-done(((bf16[1024,2048]{1,0:T(8,128)(2,1)}), bf16[256,2048]{1,0:T(8,128)(2,1)}) %reduce-scatter.2.cloned.1.call-update) | async-done | bytes 1048592 | tf_op jit(solution)/shard_map/reduce_scatter | solution.py:287
  1163.2 2.5 add_convert_fusion
  (524 shorter events, 207.9 us)
Async XLA Ops:
  6.5 8.1 copy-start.16
  6.5 793.3 %all-gather.5.cloned.1.call-start = ((), (), s32[]{:S(2)}) async-start(), calls=%async_computation.2 | async-start | bytes 5242880 | tf_op jit(solution)/shard_map/all_gather | solution.py:277
  6.6 8.9 copy-start.17
  6.6 183.9 %copy-start.9 = (pred[64,64]{1,0:T(8,128)(4,1)}, pred[64,64]{1,0:T(8,128)(4,1)S(1)}, u32[]{:S(2)}) copy-start(pred[64,64]{1,0:T(8,128)(4,1)S(1)} %get-tuple-element.490) | copy-start | bytes 12292
  6.6 8.9 copy-start.13
  10.5 7.9 copy-start.6
  12.5 344.5 %copy-start.8 = (f32[2,16,64]{2,1,0:T(8,128)}, f32[2,16,64]{2,1,0:T(8,128)S(1)}, u32[]{:S(2)}) copy-start(f32[2,16,64]{2,1,0:T(8,128)S(1)} %get-tuple-element.476) | copy-start | bytes 24580
  14.1 162.3 %copy-start.3 = (bf16[1024,2,256]{2,1,0:T(2,128)(2,1)S(1)}, bf16[1024,2,256]{2,1,0:T(2,128)(2,1)}, u32[]{:S(2)}) copy-start(bf16[1024,2,256]{2,1,0:T(2,128)(2,1)} %param.34) | copy-start | bytes 3145732
  15.4 163.4 %copy-start.19 = (pred[64,64]{1,0:T(8,128)(4,1)}, pred[64,64]{1,0:T(8,128)(4,1)S(1)}, u32[]{:S(2)}) copy-start(pred[64,64]{1,0:T(8,128)(4,1)S(1)} %get-tuple-element.492) | copy-start | bytes 12292
  176.4 2.8 copy-start.11
  183.0 4.3 copy-start
  183.0 5.3 copy-start.4
  186.3 2.8 copy-start.12
  187.3 3.2 copy-start.18
  352.9 2.1 copy-start.5
  357.0 6.8 copy-start.2
  357.0 6.8 copy-start.1
  357.0 6.8 copy-start.20
  563.7 3.4 copy-start.7
  563.7 3.4 copy-start.10
  708.7 9.3 copy-start.21
  742.0 6.1 copy-start.15
  748.1 3.4 copy-start.14
  749.3 151.4 %all-gather.7.cloned.1.call-start = ((), (), s32[]{:S(2)}) async-start(), calls=%async_computation.3 | async-start | bytes 7077888 | tf_op jit(solution)/shard_map/all_gather | solution.py:208
  750.1 249.9 %all-gather.9.cloned.1.call-start = ((), (), s32[]{:S(2)}) async-start(), calls=%async_computation.4 | async-start | bytes 7077888 | tf_op jit(solution)/shard_map/all_gather | solution.py:209
  750.8 348.2 %all-gather.11.cloned.1.call-start = ((), (), s32[]{:S(2)}) async-start(), calls=%async_computation.5 | async-start | bytes 7077888 | tf_op jit(solution)/shard_map/all_gather | solution.py:210
  751.4 411.8 %reduce-scatter.2.cloned.1.call-start = ((), (), s32[]{:S(2)}) async-start(), calls=%async_computation.6 | async-start | bytes 5242880 | tf_op jit(solution)/shard_map/reduce_scatter | solution.py:287
  910.8 1.6 copy-start.22
  912.4 186.6 %collective-permute-start = (bf16[2,1536]{1,0:T(2,128)(2,1)S(1)}, bf16[2,1536]{1,0:T(2,128)(2,1)S(1)}, u32[]{:S(2)}, u32[]{:S(2)}) collective-permute-start(bf16[2,1536]{1,0:T(2,128)(2,1)S(1)} %slice.165), channel_id=1, source_target_pairs={{0,4},{4,8},{8,12},{12,16},{16,20},{20,24},{24,28},{1,5},{5,9},{9,... | collective-permute-start | bytes 18440 | tf_op jit(solution)/shard_map/ppermute | solution.py:39
  1010.0 2.8 copy-start.23
  1010.0 89.0 %collective-permute-start.1 = (bf16[2,1536]{1,0:T(2,128)(2,1)S(1)}, bf16[2,1536]{1,0:T(2,128)(2,1)S(1)}, u32[]{:S(2)}, u32[]{:S(2)}) collective-permute-start(bf16[2,1536]{1,0:T(2,128)(2,1)S(1)} %slice.171), channel_id=1, source_target_pairs={{0,4},{4,8},{8,12},{12,16},{16,20},{20,24},{24,28},{1,5},{5,9},{9,... | collective-permute-start | bytes 18440 | tf_op jit(solution)/shard_map/ppermute | solution.py:39
Sparse Core Ops, SparseCore 0:
  749.4 50.3 all-gather.4
  802.0 98.6 all-gather.6
  902.9 96.9 all-gather.8
  1002.0 96.9 all-gather.10
  1120.4 42.7 reduce-scatter.1
where the time goes:
time: 1190 us; the launch traced here: 1170 us
  waiting for transfers between devices  365 us (31%)
  other arithmetic  337 us (28%)
  matrix products  255 us (21%)
  blocking collectives  147 us (12%)
  local copies, waits for them, and re-layouts  44.8 us (4%)
  between operations  14.3 us (1%)
    another operation x5, other arithmetic, block_terms(): lax.linalg.triangular_solve(lower + unit_mat, right_side, left_side=True,...  317 us
    all_gather x4, blocking collectives, prefix(): lax.all_gather(a.astype(kind), axis)  130 us
    all_gather x1, waiting for transfers between devices, per_device(): lax.all_gather(switching_channel_map, 'sp', axis=0, tiled=True)  101 us
    all_gather x1, waiting for transfers between devices, per_device(): lax.all_gather(narrowing_map_weights_in, 'sp', axis=0, tiled=True)  86.2 us
    all_gather x1, waiting for transfers between devices, per_device(): lax.all_gather(broadening_channel_map, 'sp', axis=0, tiled=True)  85.1 us
    all_gather x1, waiting for transfers between devices, per_device(): features = lax.all_gather(normed, 'tp', axis=0, tiled=True)  48.4 us
    reduce_scatter x1, waiting for transfers between devices, per_device(): lax.psum_scatter(lax.dot_general(hidden, whole_down, (((1,), (1,)), ((),...  42.9 us
    dot_general x32, matrix products, run_advance(): jnp.einsum('hcd,hce->hde', kdec_blk, fresh, precision=PRECISE)  38.4 us
  transfers between devices with their start and end apart: 7, of which 5 were waited for; matrix products, arithmetic and copies ran while one was open for 2% of the time, Pallas kernels for 0%

commit v1 on v0

v1 whole, which is shorter than its diff:
```python
import functools

import jax
import jax.numpy as jnp
from jax import lax
from jax.experimental import pallas as pl
from jax.experimental.pallas import tpu as pltpu
from jax.sharding import PartitionSpec as P

TAPS = 3
CHUNK = 128
BASE = 16
LANES = 128

EPSILON = 1e-06
F32 = jnp.float32
BF16 = jnp.bfloat16


def from_behind(value, axis, steps):
    count = lax.axis_size(axis)
    leading, last = (max(0, -steps), min(count, count - steps))
    return lax.ppermute(value, axis, [(source, source + steps) for source in range(leading, last)])


def mm(a, b):
    return jnp.dot(a.astype(BF16), b.astype(BF16), preferred_element_type=F32)


def mm_nt(a, b):
    return lax.dot_general(
        a.astype(BF16), b.astype(BF16), (((1,), (1,)), ((), ())), preferred_element_type=F32
    )


def mm_tn(a, b):
    return mm(a.T, b)


def local_kernel(q1_ref, k1_ref, q2_ref, k2_ref, v_ref, gb_ref, g_ref, h_ref, last_ref, run_ref):
    step = pl.program_id(0)
    count = v_ref.shape[1] // LANES // 2
    pair = LANES // (LANES // 2)
    rows = lax.broadcasted_iota(jnp.int32, (CHUNK, CHUNK), 0)
    cols = lax.broadcasted_iota(jnp.int32, (CHUNK, CHUNK), 1)
    eye = (rows == cols).astype(F32)
    causal = rows >= cols
    strict = rows > cols
    lane = lax.broadcasted_iota(jnp.int32, (1, LANES), 1)

    @pl.when(step == 0)
    def _():
        for unit in range(run_ref.shape[0]):
            run_ref[unit, :, :LANES] = jnp.zeros((LANES, LANES), F32)
            run_ref[unit, :, LANES:] = eye

    gb = gb_ref[...]
    cum = gb
    lanes8 = lax.broadcasted_iota(jnp.int32, gb.shape, 1)
    shift = 1
    while shift < CHUNK:
        cum = cum + jnp.where(lanes8 >= shift, pltpu.roll(cum, shift, 1), 0.0)
        shift *= 2
    gbt = gb.T
    cumt = cum.T

    pend = None
    for head in range(2 * count):
        group, at = head // count, head % count
        if group == 0:
            q = q1_ref[:, at * LANES : (at + 1) * LANES].astype(F32)
            k = k1_ref[:, at * LANES : (at + 1) * LANES].astype(F32)
            key_size = LANES
            own = None
        else:
            key_size = LANES // 2
            own = (lane // key_size) == at % pair
            first = (at // pair) * LANES
            q = jnp.where(own, q2_ref[:, first : first + LANES].astype(F32), 0.0)
            k = jnp.where(own, k2_ref[:, first : first + LANES].astype(F32), 0.0)
        q = q * (lax.rsqrt(jnp.sum(q * q, axis=-1, keepdims=True) + EPSILON) * key_size ** (-0.5))
        k = k * lax.rsqrt(jnp.sum(k * k, axis=-1, keepdims=True) + EPSILON)
        v = v_ref[:, head * LANES : (head + 1) * LANES].astype(F32)
        beta = gbt[:, 2 * count + head : 2 * count + head + 1]
        cum_col = cumt[:, head : head + 1]
        cum_row = cum[head : head + 1, :]
        total = cum[head : head + 1, CHUNK - 1 : CHUNK]
        decay = jnp.exp(jnp.where(causal, cum_col - cum_row, -1e30))
        grown = jnp.exp(cum_col)
        kbeta = k * beta
        kbf = k.astype(BF16)
        low = jnp.where(strict, mm_nt(kbeta, kbf) * decay, 0.0)
        intra = mm_nt(q, kbf) * decay
        base = jnp.where((rows // BASE) == (cols // BASE), low, 0.0)
        power = -base
        inv = eye + power
        size = 2
        while size < BASE:
            power = mm(power, power)
            inv = inv + mm(inv, power)
            size *= 2
        block = BASE
        while block < CHUNK:
            off = jnp.where(
                ((rows // (2 * block)) == (cols // (2 * block)))
                & ((rows // block) != (cols // block)),
                low,
                0.0,
            )
            inv = inv - mm(mm(inv, off), inv)
            block *= 2
        right = jnp.concatenate([v * beta, kbeta * grown], axis=-1)
        solved = mm(inv, right)
        kdec = k * jnp.exp(total - cum_col)
        both = mm_tn(kdec, solved)
        inner = mm(intra, solved)
        unit_diag = eye if own is None else jnp.where(own, eye, 0.0)
        cmap = jnp.exp(total) * unit_diag - both[:, LANES:]
        cadd = both[:, :LANES]
        pmat = q * grown - inner[:, LANES:]
        unit = head if group == 0 else count + at // pair
        run = run_ref[unit]
        seen = mm(pmat, run)
        h_ref[:, head * LANES : (head + 1) * LANES] = seen[:, :LANES] + inner[:, :LANES]
        g_ref[:, head * LANES : (head + 1) * LANES] = seen[:, LANES:].astype(g_ref.dtype)
        if pend is not None:
            cmap = cmap + pend[0]
            cadd = cadd + pend[1]
            pend = None
        if group == 1 and at % pair != pair - 1 and at != count - 1:
            pend = (cmap, cadd)
            continue
        nxt = mm(cmap, run)
        run_ref[unit, :, :LANES] = nxt[:, :LANES] + cadd
        run_ref[unit, :, LANES:] = nxt[:, LANES:]

    @pl.when(step == pl.num_programs(0) - 1)
    def _():
        last_ref[...] = run_ref[...].astype(last_ref.dtype)


def local_terms(q1, k1, q2, k2, values, gates_beta):
    length = q1.shape[0]
    wide = values.shape[1]
    steps = length // CHUNK
    units = q1.shape[1] // LANES + q2.shape[1] // LANES
    return pl.pallas_call(
        local_kernel,
        grid=(steps,),
        in_specs=[
            pl.BlockSpec((CHUNK, q1.shape[1]), lambda i: (i, 0)),
            pl.BlockSpec((CHUNK, k1.shape[1]), lambda i: (i, 0)),
            pl.BlockSpec((CHUNK, q2.shape[1]), lambda i: (i, 0)),
            pl.BlockSpec((CHUNK, k2.shape[1]), lambda i: (i, 0)),
            pl.BlockSpec((CHUNK, wide), lambda i: (i, 0)),
            pl.BlockSpec((gates_beta.shape[0], CHUNK), lambda i: (0, i)),
        ],
        out_specs=[
            pl.BlockSpec((CHUNK, wide), lambda i: (i, 0)),
            pl.BlockSpec((CHUNK, wide), lambda i: (i, 0)),
            pl.BlockSpec((units, LANES, 2 * LANES), lambda i: (0, 0, 0)),
        ],
        out_shape=[
            jax.ShapeDtypeStruct((length, wide), BF16),
            jax.ShapeDtypeStruct((length, wide), F32),
            jax.ShapeDtypeStruct((units, LANES, 2 * LANES), BF16),
        ],
        scratch_shapes=[pltpu.VMEM((units, LANES, 2 * LANES), F32)],
        cost_estimate=pl.CostEstimate(
            flops=steps * 4 * 60 * CHUNK**3, bytes_accessed=length * wide * 10, transcendentals=0
        ),
    )(q1, k1, q2, k2, values, gates_beta)


def finish_kernel(place_ref, all_ref, g_ref, h_ref, gate_ref, coef_ref, out_ref, state_ref):
    @pl.when(pl.program_id(0) == 0)
    def _():
        state_ref[...] = jnp.zeros_like(state_ref)

        def turn(i, carry):
            for unit in range(all_ref.shape[1]):
                block = all_ref[i, unit]
                state_ref[unit] = (
                    mm(block[:, LANES:], state_ref[unit]) + block[:, :LANES].astype(F32)
                )
            return carry

        lax.fori_loop(0, place_ref[0], turn, 0)

    coef = coef_ref[...]
    count = out_ref.shape[1] // LANES // 2
    for head in range(2 * count):
        unit = head if head < count else count + (head - count) // 2
        at = pl.ds(head * LANES, LANES)
        out = mm(g_ref[:, at], state_ref[unit]) + h_ref[:, at]
        gate = gate_ref[:, at].astype(F32)
        scaled = out * lax.rsqrt(jnp.mean(out * out, axis=-1, keepdims=True) + EPSILON) * coef
        out_ref[:, at] = (scaled * (gate / (1.0 + jnp.exp(-gate)))).astype(out_ref.dtype)


def finish_heads(place, everyone, g, h, gates, coef):
    length, wide = g.shape
    tile = min(256, length)
    return pl.pallas_call(
        finish_kernel,
        grid_spec=pltpu.PrefetchScalarGridSpec(
            num_scalar_prefetch=1,
            grid=(length // tile,),
            in_specs=[
                pl.BlockSpec(everyone.shape, lambda i, p: (0, 0, 0, 0)),
                pl.BlockSpec((tile, wide), lambda i, p: (i, 0)),
                pl.BlockSpec((tile, wide), lambda i, p: (i, 0)),
                pl.BlockSpec((tile, wide), lambda i, p: (i, 0)),
                pl.BlockSpec((1, LANES), lambda i, p: (0, 0)),
            ],
            out_specs=pl.BlockSpec((tile, wide), lambda i, p: (i, 0)),
            scratch_shapes=[pltpu.VMEM((everyone.shape[1], LANES, LANES), F32)],
        ),
        out_shape=jax.ShapeDtypeStruct((length, wide), BF16),
        cost_estimate=pl.CostEstimate(
            flops=2 * length * wide * LANES * 8, bytes_accessed=length * wide * 10, transcendentals=0
        ),
    )(place, everyone, g, h, gates, coef)


def causal_taps(edge_rows, low_rows, taps_col):
    padded = jnp.concatenate([edge_rows, low_rows], axis=0)
    length = low_rows.shape[0]
    total = taps_col[0] * padded[0:length]
    for tap_index in range(1, TAPS):
        total = total + taps_col[tap_index] * padded[tap_index : tap_index + length]
    return total


def per_device(
    arriving_hidden_state,
    former_request_vectors,
    former_match_vectors,
    latter_request_vectors,
    latter_match_vectors,
    stored_vectors_both,
    closing_valve_operands,
    update_level_before_squash,
    fading_data_input,
    sparse_fading_boost,
    unitwise_fading_loglevel,
    fading_constant_term,
    unitwise_normalizer_coef,
    emission_map_weights,
    channel_normalizer_coef,
    switching_channel_map,
    broadening_channel_map,
    timewise_convolve_tapvalues,
    narrowing_map_weights_in,
):
    whole_gate, whole_up, whole_down = (
        lax.all_gather(switching_channel_map, "sp", axis=0, tiled=True),
        lax.all_gather(broadening_channel_map, "sp", axis=0, tiled=True),
        lax.all_gather(narrowing_map_weights_in, "sp", axis=0, tiled=True),
    )
    length = former_request_vectors.shape[0]
    level = (
        -jnp.exp(unitwise_fading_loglevel)[..., None]
        * jax.nn.softplus(fading_data_input + fading_constant_term[..., None])
        + sparse_fading_boost
    )
    beta_rate = jax.nn.sigmoid(update_level_before_squash.astype(jnp.float32))
    gates_beta = jnp.concatenate([level, beta_rate], axis=0).reshape(-1, length)
    gates_beta = jnp.pad(gates_beta, ((0, -gates_beta.shape[0] % 8), (0, 0)))
    spare = -latter_request_vectors.shape[1] % LANES
    g_part, h_part, summary = local_terms(
        former_request_vectors,
        former_match_vectors,
        jnp.pad(latter_request_vectors, ((0, 0), (0, spare))),
        jnp.pad(latter_match_vectors, ((0, 0), (0, spare))),
        stored_vectors_both.reshape(length, -1),
        gates_beta,
    )
    everyone = lax.all_gather(summary, "sp")
    place = lax.axis_index("sp").astype(jnp.int32).reshape(1)
    attended = finish_heads(
        place,
        everyone,
        g_part,
        h_part,
        closing_valve_operands.reshape(length, -1),
        unitwise_normalizer_coef.reshape(1, -1),
    )
    linear_attend = attended.reshape(length, 2, -1)
    arrived = lax.all_to_all(linear_attend, "tp", split_axis=0, concat_axis=2, tiled=True)
    row_count = arrived.shape[0]
    skip_stream = arriving_hidden_state.astype(jnp.float32) + jnp.dot(
        arrived.reshape(row_count, -1), emission_map_weights, preferred_element_type=jnp.float32
    )
    normed = (
        skip_stream
        * lax.rsqrt(jnp.mean(skip_stream * skip_stream, axis=-1, keepdims=True) + EPSILON)
        * channel_normalizer_coef
    ).astype(jnp.bfloat16)
    features = lax.all_gather(normed, "tp", axis=0, tiled=True)
    gate_full = jnp.dot(features, whole_gate, preferred_element_type=jnp.float32)
    up_full = jnp.dot(features, whole_up, preferred_element_type=jnp.float32)
    gate_low = gate_full.astype(jnp.bfloat16)
    up_low = up_full.astype(jnp.bfloat16)
    edge_gate, edge_up = from_behind((gate_low[-(TAPS - 1) :], up_low[-(TAPS - 1) :]), "sp", 1)
    taps = timewise_convolve_tapvalues.astype(jnp.float32)
    gate_conv = causal_taps(edge_gate, gate_low, taps[:, 0])
    up_conv = causal_taps(edge_up, up_low, taps[:, 1])
    hidden = (jax.nn.silu(gate_conv) * up_conv).astype(jnp.bfloat16)
    down_sum = lax.psum_scatter(
        lax.dot_general(
            hidden, whole_down, (((1,), (1,)), ((), ())), preferred_element_type=jnp.float32
        ).astype(jnp.bfloat16),
        "tp",
        scatter_dimension=0,
        tiled=True,
    ).astype(jnp.float32)
    return (skip_stream + down_sum).astype(jnp.bfloat16)


def solution(mesh):
    placed = (
        P(("sp", "tp"), None),
        P("sp", "tp"),
        P("sp", "tp"),
        P("sp", "tp"),
        P("sp", "tp"),
        P("sp", None, "tp"),
        P("sp", None, "tp"),
        P(None, "tp", "sp"),
        P(None, "tp", "sp"),
        P(None, "tp", "sp"),
        P(None, "tp"),
        P(None, "tp"),
        P(),
        P(),
        P(),
        P("sp", "tp"),
        P("sp", "tp"),
        P(None, None, "tp"),
        P("sp", "tp"),
    )
    return jax.shard_map(
        per_device, mesh=mesh, in_specs=placed, out_specs=P(("sp", "tp"), None), check_vma=False
    )
```

time: 1190 us -> 558 us (0.47); the launches traced: 1170 us -> 558 us
  other arithmetic: 337 us -> 5.27 us
  matrix products: 255 us -> 47.2 us
  blocking collectives: 147 us -> 17 us
  Pallas kernels: 0 us -> 67.7 us
  local copies, waits for them, and re-layouts: 44.8 us -> 8 us
  waiting for transfers between devices: 365 us -> 394 us
    another operation x8 -> x0, other arithmetic: 318 us -> none  [the longest x5 317 us: block_terms(): lax.linalg.triangular_solve(lower + unit_mat, right_side, left_side=True,...]
    dot_general x200 -> x0, matrix products: 204 us -> none  [the longest x32 38.4 us: run_advance(): jnp.einsum('hcd,hce->hde', kdec_blk, fresh, precision=PRECISE)]
    all_gather x4 -> x0, blocking collectives: 130 us -> none  [prefix(): lax.all_gather(a.astype(kind), axis)]
    pallas_call x0 -> x2, Pallas kernels: none -> 67.7 us  [the longest x1 62.2 us: local_terms(): pl.pallas_call(local_kernel, grid=(steps,), in_specs=[pl.BlockSpec((CHUNK...]
    all_gather x0 -> x1, waiting for transfers between devices: none -> 45.8 us  [per_device(): everyone = lax.all_gather(summary, 'sp')]
    all_gather x1, waiting for transfers between devices: 48.4 us -> 31.2 us  [per_device(): features = lax.all_gather(normed, 'tp', axis=0, tiled=True)]
  transfers between devices with their start and end apart: 7 -> 8, of which waited for: 5 -> 6; matrix products, arithmetic and copies ran while one was open for 2% -> 4% of each run, Pallas kernels for 0% -> 0%
where the time goes in v1:
time: 558 us
  waiting for transfers between devices  394 us (71%)
  Pallas kernels  67.7 us (12%)
  matrix products  47.2 us (8%)
  blocking collectives  17 us (3%)
  between operations  13.6 us (2%)
  local copies, waits for them, and re-layouts  8 us (1%)
    all_gather x1, waiting for transfers between devices, per_device(): lax.all_gather(switching_channel_map, 'sp', axis=0, tiled=True)  101 us
    all_gather x1, waiting for transfers between devices, per_device(): lax.all_gather(narrowing_map_weights_in, 'sp', axis=0, tiled=True)  86.4 us
    all_gather x1, waiting for transfers between devices, per_device(): lax.all_gather(broadening_channel_map, 'sp', axis=0, tiled=True)  84.8 us
    pallas_call x1, Pallas kernels, local_terms(): pl.pallas_call(local_kernel, grid=(steps,), in_specs=[pl.BlockSpec((CHUNK...  62.2 us
    all_gather x1, waiting for transfers between devices, per_device(): everyone = lax.all_gather(summary, 'sp')  45.8 us
    reduce_scatter x1, waiting for transfers between devices, per_device(): lax.psum_scatter(lax.dot_general(hidden, whole_down, (((1,), (1,)), ((),...  42.9 us
    all_gather x1, waiting for transfers between devices, per_device(): features = lax.all_gather(normed, 'tp', axis=0, tiled=True)  31.2 us
    dot_general x1, matrix products, per_device(): lax.dot_general(hidden, whole_down, (((1,), (1,)), ((), ())), preferred_e...  21.1 us
  transfers between devices with their start and end apart: 8, of which 6 were waited for; matrix products, arithmetic and copies ran while one was open for 4% of the time, Pallas kernels for 0%

profile of v1, /device:TPU:0, one launch (start us, length us, event | category | flops | bytes accessed | tf_op | source)
XLA Modules:
  0.0 557.9 jit_solution(16485203441814309797)
XLA Ops:
  6.5 0.0 all-gather.15.cloned.1.call-start
  6.5 0.7 exponential_negate_fusion
  7.2 0.9 fusion.3
  8.1 0.6 reshape.48.gb_ref
  8.7 2.4 copy.24
  11.2 62.2 %shard_map.181 = (bf16[1024,512]{1,0:T(8,128)(2,1)}, f32[1024,512]{1,0:T(8,128)}, bf16[3,128,256]{2,1,0:T(8,128)(2,1)}) custom-call(bf16[1024,256]{1,0:T(8,128)(2,1)} %q1_ref.1, bf16[1024,256]{1,0:T(8,128)(2,1)} %k1_ref.1, bf16[1024,128]{1,0:T(8,128)(2,1)} %q2_ref.1, bf16[1024,128]{1,0:T(8,128)(2,1)} %k2_ref.1, bf16[1024,512]{1,0:T(8,128)(2,1)} %bitcast.24, ...), custom_call_target="tpu_custom_call" | custom-call | flops 4026531840 | bytes 5242880 | tf_op jit(solution)/shard_map/pallas_call | solution.py:147
  73.4 0.0 all-gather.15.cloned.1.call-update
  73.4 0.0 all-gather.7.cloned.1.call-start
  73.5 0.0 copy-done
  73.5 1.2 copy.25
  74.7 45.8 %all-gather.15.cloned.1.call-done = bf16[24,128,256]{2,1,0:T(8,128)(2,1)} async-done(((bf16[3,128,256]{2,1,0:T(8,128)(2,1)}), bf16[24,128,256]{2,1,0:T(8,128)(2,1)}) %all-gather.15.cloned.1.call-update) | async-done | bytes 1572880 | tf_op jit(solution)/shard_map/all_gather | solution.py:279
  120.5 5.5 shard_map.182
  126.0 1.3 reshape.51
  127.3 17.0 %all_to_all.15 = bf16[1024,2,256]{2,1,0:T(2,128)(2,1)S(1)} all-to-all(bf16[1024,2,256]{2,1,0:T(2,128)(2,1)S(1)} %reshape.51), channel_id=1, replica_groups=mesh['sp'=8,'tp'=4] {'tp'}, dimensions={0} | all-to-all | bytes 2097152 | tf_op jit(solution)/shard_map/all_to_all | solution.py:290
  144.3 0.1 copy.22
  144.4 0.5 copy.23
  144.9 0.0 copy-start.2
  145.0 6.1 %multiply_reduce_fusion = (f32[256]{0:T(256)S(1)}, f32[256,2048]{1,0:T(8,128)S(1)}) fusion(bf16[256,2048]{0,1:T(8,128)(2,1)S(1)} %bitcast.18, bf16[2048,2048]{1,0:T(8,128)(2,1)} %param.32, bf16[256,2048]{1,0:T(8,128)(2,1)} %param.19), kind=kOutput, calls=%fused_computation.15 | convolution fusion | flops 2149580544 | bytes 12583936 | tf_op jit(solution)/shard_map/dot_general | solution.py:292
  151.0 0.0 copy-start.1
  151.0 0.0 copy-done.2
  151.1 1.2 multiply_convert_fusion.2
  152.3 0.0 all-gather.7.cloned.1.call-update
  152.3 0.0 all-gather.9.cloned.1.call-start
  152.3 0.7 all-gather.9.cloned.1.call-update
  153.0 0.0 all-gather.11.cloned.1.call-start
  153.1 0.5 all-gather.11.cloned.1.call-update
  153.6 0.0 all-gather.13.cloned.1.call-start
  153.7 0.5 all-gather.13.cloned.1.call-update
  154.2 0.0 reduce-scatter.2.cloned.1.call-start
  154.2 0.0 copy-done.1
  154.3 31.2 %all-gather.7.cloned.1.call-done = bf16[1024,2048]{1,0:T(8,128)(2,1)} async-done(((bf16[256,2048]{1,0:T(8,128)(2,1)}), bf16[1024,2048]{1,0:T(8,128)(2,1)}) %all-gather.7.cloned.1.call-update) | async-done | bytes 4194320 | tf_op jit(solution)/shard_map/all_gather | solution.py:300
  185.5 100.9 %all-gather.9.cloned.1.call-done = bf16[2048,1536]{1,0:T(8,128)(2,1)} async-done(((bf16[256,1536]{1,0:T(8,128)(2,1)}), bf16[2048,1536]{1,0:T(8,128)(2,1)}) %all-gather.9.cloned.1.call-update) | async-done | bytes 6291472 | tf_op jit(solution)/shard_map/all_gather | solution.py:257
  286.4 10.0 %convolution_convert_fusion.2 = bf16[1024,1536]{1,0:T(8,128)(2,1)S(1)} fusion(bf16[1024,2048]{1,0:T(8,128)(2,1)} %all-gather.7.cloned.1.call-done, bf16[2048,1536]{1,0:T(8,128)(2,1)} %all-gather.9.cloned.1.call-done), kind=kOutput, calls=%fused_computation.3 | convolution fusion | flops 6444023808 | bytes 13631488 | tf_op jit(solution)/shard_map/dot_general | solution.py:301
  296.4 0.0 copy-start.3
  296.5 1.6 copy-done.3
  298.1 2.6 collective-permute-start
  300.7 84.8 %all-gather.11.cloned.1.call-done = bf16[2048,1536]{1,0:T(8,128)(2,1)} async-done(((bf16[256,1536]{1,0:T(8,128)(2,1)}), bf16[2048,1536]{1,0:T(8,128)(2,1)}) %all-gather.11.cloned.1.call-update) | async-done | bytes 6291472 | tf_op jit(solution)/shard_map/all_gather | solution.py:258
  385.5 10.0 %convolution_convert_fusion.1 = bf16[1024,1536]{1,0:T(8,128)(2,1)S(1)} fusion(bf16[1024,2048]{1,0:T(8,128)(2,1)} %all-gather.7.cloned.1.call-done, bf16[2048,1536]{1,0:T(8,128)(2,1)} %all-gather.11.cloned.1.call-done), kind=kOutput, calls=%fused_computation.2 | convolution fusion | flops 6444023808 | bytes 13631488 | tf_op jit(solution)/shard_map/dot_general | solution.py:302
  395.5 0.0 copy-start.4
  395.5 2.5 collective-permute-start.1
  398.0 0.1 slice_reduce_fusion.5
  398.1 86.4 %all-gather.13.cloned.1.call-done = bf16[2048,1536]{1,0:T(8,128)(2,1)} async-done(((bf16[256,1536]{1,0:T(8,128)(2,1)}), bf16[2048,1536]{1,0:T(8,128)(2,1)}) %all-gather.13.cloned.1.call-update) | async-done | bytes 6291472 | tf_op jit(solution)/shard_map/all_gather | solution.py:259
  484.6 0.0 collective-permute-done
  484.6 0.0 collective-permute-done.1
  484.6 21.1 %convolution_convert_fusion = bf16[1024,2048]{1,0:T(8,128)(2,1)} fusion(bf16[2048,1536]{1,0:T(8,128)(2,1)} %all-gather.13.cloned.1.call-done, bf16[1024,1536]{1,0:T(8,128)(2,1)} %copy-done.4, bf16[1024,1536]{1,0:T(8,128)(2,1)} %copy-done.3, bf16[2,1536]{1,0:T(2,128)(2,1)S(1)} %collective-permute-done.1, bf16[2,1536]{1,0:T(2,128)(2,1)S(1)} %collective-permute-done, ...), kind=kOutput, calls=%fused_computation.1 | convolution fusion | flops 6498025472 | bytes 16826368 | tf_op jit(solution)/shard_map/dot_general | solution.py:311
  505.7 0.0 reduce-scatter.2.cloned.1.call-update
  505.7 42.9 %reduce-scatter.2.cloned.1.call-done = bf16[256,2048]{1,0:T(8,128)(2,1)} async-done(((bf16[1024,2048]{1,0:T(8,128)(2,1)}), bf16[256,2048]{1,0:T(8,128)(2,1)}) %reduce-scatter.2.cloned.1.call-update) | async-done | bytes 1048592 | tf_op jit(solution)/shard_map/reduce_scatter | solution.py:310
  548.6 2.5 add_convert_fusion
  (7 shorter events, 0.1 us)
Async XLA Ops:
  6.5 113.9 %all-gather.15.cloned.1.call-start = ((), (), s32[]{:S(2)}) async-start(), calls=%async_computation.7 | async-start | bytes 1769472 | tf_op jit(solution)/shard_map/all_gather | solution.py:279
  11.2 62.3 %copy-start = (bf16[1024,2,256]{2,1,0:T(2,128)(2,1)S(1)}, bf16[1024,2,256]{2,1,0:T(2,128)(2,1)}, u32[]{:S(2)}) copy-start(bf16[1024,2,256]{2,1,0:T(2,128)(2,1)} %param.25) | copy-start | bytes 3145732
  73.4 112.1 %all-gather.7.cloned.1.call-start = ((), (), s32[]{:S(2)}) async-start(), calls=%async_computation.2 | async-start | bytes 5242880 | tf_op jit(solution)/shard_map/all_gather | solution.py:300
  144.9 6.1 %copy-start.2 = (f32[2048]{0:T(1024)S(1)}, f32[2048]{0:T(1024)}, u32[]{:S(2)}) copy-start(f32[2048]{0:T(1024)} %param.33) | copy-start | bytes 24580
  151.0 3.2 copy-start.1
  152.3 134.1 %all-gather.9.cloned.1.call-start = ((), (), s32[]{:S(2)}) async-start(), calls=%async_computation.3 | async-start | bytes 7077888 | tf_op jit(solution)/shard_map/all_gather | solution.py:257
  153.0 232.5 %all-gather.11.cloned.1.call-start = ((), (), s32[]{:S(2)}) async-start(), calls=%async_computation.4 | async-start | bytes 7077888 | tf_op jit(solution)/shard_map/all_gather | solution.py:258
  153.6 331.0 %all-gather.13.cloned.1.call-start = ((), (), s32[]{:S(2)}) async-start(), calls=%async_computation.5 | async-start | bytes 7077888 | tf_op jit(solution)/shard_map/all_gather | solution.py:259
  154.2 394.4 %reduce-scatter.2.cloned.1.call-start = ((), (), s32[]{:S(2)}) async-start(), calls=%async_computation.6 | async-start | bytes 5242880 | tf_op jit(solution)/shard_map/reduce_scatter | solution.py:310
  296.4 1.6 copy-start.3
  298.1 186.5 %collective-permute-start = (bf16[2,1536]{1,0:T(2,128)(2,1)S(1)}, bf16[2,1536]{1,0:T(2,128)(2,1)S(1)}, u32[]{:S(2)}, u32[]{:S(2)}) collective-permute-start(bf16[2,1536]{1,0:T(2,128)(2,1)S(1)} %slice.63), channel_id=1, source_target_pairs={{0,4},{4,8},{8,12},{12,16},{16,20},{20,24},{24,28},{1,5},{5,9},{9,... | collective-permute-start | bytes 18440 | tf_op jit(solution)/shard_map/ppermute | solution.py:23
  395.5 2.5 copy-start.4
  395.5 89.0 %collective-permute-start.1 = (bf16[2,1536]{1,0:T(2,128)(2,1)S(1)}, bf16[2,1536]{1,0:T(2,128)(2,1)S(1)}, u32[]{:S(2)}, u32[]{:S(2)}) collective-permute-start(bf16[2,1536]{1,0:T(2,128)(2,1)S(1)} %slice.69), channel_id=1, source_target_pairs={{0,4},{4,8},{8,12},{12,16},{16,20},{20,24},{24,28},{1,5},{5,9},{9,... | collective-permute-start | bytes 18440 | tf_op jit(solution)/shard_map/ppermute | solution.py:23
Sparse Core Ops, SparseCore 0:
  73.5 46.8 all-gather.14
  152.4 33.0 all-gather.6
  187.7 98.6 all-gather.8
  288.5 96.9 all-gather.10
  387.5 96.9 all-gather.12
  505.8 42.7 reduce-scatter.1
